TPU v7x, 32 devices: a whole 2x2x4 slice. The times are simulated.
32 devices in a mesh: ep: 8 (over z, y), tp: 4 (over x, core).
Axes of the slice: x: 2, y: 2, z: 4, core: 2. Of those that a mesh axis runs over, the one named last changes fastest.
Arguments:
- hidden: bfloat16 [256, 2048], P('ep')
- norm_gains: float32 [4, 2048], replicated, may hold values from 0.1 to 1.9
- w_query: bfloat16 [2048, 1024], P(None, 'tp'), may hold values from -0.125 to 0.125
- w_key: bfloat16 [2048, 1024], P(None, 'tp'), may hold values from -0.125 to 0.125
- w_value: bfloat16 [2048, 1024], P(None, 'tp'), may hold values from -0.125 to 0.125
- w_outgate: bfloat16 [2048, 1024], P(None, 'tp'), may hold values from -0.125 to 0.125
- w_input_gate: bfloat16 [2048, 8], replicated, may hold values from -0.125 to 0.125
- w_forget_gate: bfloat16 [2048, 8], replicated, may hold values from -0.125 to 0.125
- forget_bias: float32 [8], replicated, may hold values from -1 to 4
- w_mix_out: bfloat16 [1024, 2048], P('tp')
- state_matrix: float32 [256, 8, 128, 128], P('ep', 'tp'), may hold values from -0.6 to 0.6
- state_norm: float32 [256, 8, 128], P('ep', 'tp'), may hold values from -0.6 to 0.6
- state_max: float32 [256, 8], P('ep', 'tp'), may hold values from -4 to 4
- routes: int32 [256, 2], P('ep'), may hold values from 0 to 7, all different within a row; in each aligned block of 32 rows (0 to 31, 32 to 63, ...) at most 16 rows name the same one
- route_scores: float32 [256, 2], P('ep'), may hold values from 0.1 to 1
- expert_gate: bfloat16 [8, 2048, 3584], P('ep', None, 'tp'), may hold values from -0.125 to 0.125
- expert_up: bfloat16 [8, 2048, 3584], P('ep', None, 'tp'), may hold values from -0.125 to 0.125
- expert_down: bfloat16 [8, 3584, 2048], P('ep', 'tp')
- dense_gate: bfloat16 [2048, 5632], P('tp', 'ep'), may hold values from -0.125 to 0.125
- dense_up: bfloat16 [2048, 5632], P('tp', 'ep'), may hold values from -0.125 to 0.125
- dense_down: bfloat16 [5632, 2048], P('ep', 'tp')
- dense_mix: float32 [2048], replicated, may hold values from -0.25 to 0.25
Outputs:
- new_hidden: bfloat16 [256, 2048], P('ep', 'tp')
- new_matrix: float32 [256, 8, 128, 128], P('ep', 'tp')
- new_norm: float32 [256, 8, 128], P('ep', 'tp')
- new_max: float32 [256, 8], P('ep', 'tp')
Inputs may be any that keep to these rules, and one draw needn't show every extreme that they name: `routes`: each row names 2 different experts. Among the rows of one index of ep (an aligned block of 32 rows) no expert is named by more than 16 rows, and in every draw some expert is named by exactly 16 rows of some block.
All inputs are finite; a program needn't handle non-finite values.
Results may differ from a plain program's by a relative error of at most 0.02.
Values may be sent and summed in bfloat16 or wider, within the bound.
No kernel may reach another device: no remote copies, remote signals or barrier semaphores. Data moves between devices by JAX's collectives and lax.ppermute only.
A program may use at most 128 MiB of HBM per device.

v0:
```python
import jax
import jax.numpy as jnp
from jax import lax
from jax.sharding import PartitionSpec as P

EPS = 1e-06


def settle(values):
    return lax.optimization_barrier(values.astype(jnp.bfloat16)).astype(jnp.float32)


def local(
    hidden,
    norm_gains,
    w_query,
    w_key,
    w_value,
    w_outgate,
    w_input_gate,
    w_forget_gate,
    forget_bias,
    w_mix_out,
    state_matrix,
    state_norm,
    state_max,
    routes,
    route_scores,
    expert_gate,
    expert_up,
    expert_down,
    dense_gate,
    dense_up,
    dense_down,
    dense_mix,
):
    tp_count = lax.axis_size("tp")
    ep_count = lax.axis_size("ep")
    tp_place = lax.axis_index("tp")
    seq_local, width = hidden.shape
    heads_local = state_matrix.shape[1]
    head_width = state_matrix.shape[2]
    part_width = width // tp_count
    feature_first = tp_place * part_width
    start_f = hidden.astype(jnp.float32)
    normed_in = (
        start_f
        * lax.rsqrt(jnp.mean(start_f * start_f, axis=-1, keepdims=True) + EPS)
        * norm_gains[0]
    ).astype(jnp.bfloat16)
    query_f = jnp.dot(normed_in, w_query, preferred_element_type=jnp.float32)
    key_f = jnp.dot(normed_in, w_key, preferred_element_type=jnp.float32)
    value_f = jnp.dot(normed_in, w_value, preferred_element_type=jnp.float32)
    gate_f = jnp.dot(normed_in, w_outgate, preferred_element_type=jnp.float32)
    head_first = tp_place * heads_local
    input_weight = lax.dynamic_slice_in_dim(w_input_gate, head_first, heads_local, 1)
    forget_weight = lax.dynamic_slice_in_dim(w_forget_gate, head_first, heads_local, 1)
    forget_local = lax.dynamic_slice_in_dim(forget_bias, head_first, heads_local, 0)
    in_gate = jnp.dot(normed_in, input_weight, preferred_element_type=jnp.float32)
    log_forget = jax.nn.log_sigmoid(
        jnp.dot(normed_in, forget_weight, preferred_element_type=jnp.float32) + forget_local
    )
    query = settle(query_f).reshape(seq_local, heads_local, head_width)
    keys = settle(key_f).reshape(seq_local, heads_local, head_width) * head_width ** (-0.5)
    values = settle(value_f).reshape(seq_local, heads_local, head_width)
    carried = log_forget + state_max
    new_max = jnp.maximum(carried, in_gate)
    keep = jnp.exp(carried - new_max)
    write = jnp.exp(in_gate - new_max)
    written = write[:, :, None] * keys
    new_matrix = (
        keep[:, :, None, None] * state_matrix + written[:, :, :, None] * values[:, :, None, :]
    )
    new_norm = keep[:, :, None] * state_norm + written
    numer = jnp.einsum("shd,shdv->shv", query, new_matrix)
    denom = jnp.einsum("shd,shd->sh", query, new_norm)
    read = numer / jnp.maximum(jnp.abs(denom), jnp.exp(-new_max))[:, :, None]
    mixed = (
        jax.nn.sigmoid(settle(gate_f)) * read.reshape(seq_local, heads_local * head_width)
    ).astype(jnp.bfloat16)
    branch_terms = settle(jnp.dot(mixed, w_mix_out, preferred_element_type=jnp.float32))
    branch = settle(
        lax.psum_scatter(
            branch_terms.astype(jnp.bfloat16), "tp", scatter_dimension=1, tiled=True
        ).astype(jnp.float32)
    )
    start_part = lax.dynamic_slice_in_dim(start_f, feature_first, part_width, 1)
    gain_rows = lax.dynamic_slice_in_dim(norm_gains, feature_first, part_width, 1)
    lifted = gain_rows[1] * branch
    mix_weight = gain_rows[2] * lax.dynamic_slice_in_dim(dense_mix, feature_first, part_width, 0)
    branch_sq, start_sq, cross_sum, lifted_sq, start_dot, lifted_dot = lax.psum(
        (
            jnp.sum(branch * branch, axis=-1),
            jnp.sum(start_part * start_part, axis=-1),
            jnp.sum(start_part * lifted, axis=-1),
            jnp.sum(lifted * lifted, axis=-1),
            jnp.sum(start_part * mix_weight, axis=-1),
            jnp.sum(lifted * mix_weight, axis=-1),
        ),
        "tp",
    )
    branch_scale = lax.rsqrt(branch_sq / width + EPS)
    residual_f = start_part + lifted * branch_scale[:, None]
    resid_sq = start_sq + 2.0 * branch_scale * cross_sum + branch_scale * branch_scale * lifted_sq
    gate_dot = start_dot + branch_scale * lifted_dot
    scale_two = lax.rsqrt(resid_sq / width + EPS)
    mix_gate = jax.nn.sigmoid(scale_two * gate_dot)
    residual = settle(residual_f)
    normed = (residual_f * scale_two[:, None] * gain_rows[2]).astype(jnp.bfloat16)
    rows_in = lax.all_gather(normed, "ep", axis=0, tiled=True)
    dense_pre = jnp.concatenate(
        [
            jnp.dot(rows_in, dense_gate, preferred_element_type=jnp.float32),
            jnp.dot(rows_in, dense_up, preferred_element_type=jnp.float32),
        ],
        axis=1,
    )
    dense_pre = lax.psum(dense_pre.astype(jnp.bfloat16), "tp").astype(jnp.float32)
    dense_pre_gate, dense_pre_up = jnp.split(dense_pre, 2, axis=1)
    dense_hidden = (jax.nn.silu(dense_pre_gate) * dense_pre_up).astype(jnp.bfloat16)
    dense_out = lax.psum_scatter(
        jnp.dot(dense_hidden, dense_down, preferred_element_type=jnp.float32).astype(jnp.bfloat16),
        "ep",
        scatter_dimension=0,
        tiled=True,
    ).astype(jnp.float32)
    route_width = routes.shape[1]
    expert_count = ep_count * expert_gate.shape[0]
    capacity = 2 * seq_local * route_width // ep_count
    flat_expert = routes.reshape(-1)
    picks = (flat_expert[:, None] == jnp.arange(expert_count, dtype=jnp.int32)[None, :]).astype(
        jnp.int32
    )
    ranks = jnp.sum(jnp.cumsum(picks, axis=0) * picks, axis=1) - 1
    slot_index = flat_expert * capacity + ranks
    placing = (
        jnp.arange(expert_count * capacity, dtype=jnp.int32)[:, None] == slot_index[None, :]
    ).astype(jnp.bfloat16)
    repeated = jnp.repeat(normed, route_width, axis=0)
    outgoing = (
        jnp.dot(placing, repeated, preferred_element_type=jnp.float32)
        .astype(jnp.bfloat16)
        .reshape(expert_count, capacity, part_width)
    )
    arrived = lax.all_to_all(outgoing, "ep", split_axis=0, concat_axis=0, tiled=True)
    full_rows = lax.all_gather(arrived, "tp", axis=2, tiled=True)
    flat_rows = full_rows.reshape(-1, width)
    gate_pre = jnp.dot(flat_rows, expert_gate[0], preferred_element_type=jnp.float32)
    up_pre = jnp.dot(flat_rows, expert_up[0], preferred_element_type=jnp.float32)
    hidden_units = (jax.nn.silu(gate_pre) * up_pre).astype(jnp.bfloat16)
    partial_out = settle(jnp.dot(hidden_units, expert_down[0], preferred_element_type=jnp.float32))
    summed_out = lax.psum_scatter(
        partial_out.astype(jnp.bfloat16), "tp", scatter_dimension=1, tiled=True
    )
    returned = lax.all_to_all(
        summed_out.reshape(arrived.shape), "ep", split_axis=0, concat_axis=0, tiled=True
    )
    picked = lax.dot_general(
        placing,
        returned.reshape(expert_count * capacity, part_width),
        (((0,), (0,)), ((), ())),
        preferred_element_type=jnp.float32,
    )
    share = route_scores / jnp.sum(route_scores, axis=-1, keepdims=True)
    moe_out = jnp.sum(
        picked.reshape(seq_local, route_width, part_width) * share[:, :, None], axis=1
    )
    ffn = moe_out + mix_gate[:, None] * dense_out
    ffn_sq = lax.psum(jnp.sum(ffn * ffn, axis=-1), "tp")
    new_hidden = (residual + gain_rows[3] * ffn * lax.rsqrt(ffn_sq / width + EPS)[:, None]).astype(
        jnp.bfloat16
    )
    return (new_hidden, new_matrix, new_norm, new_max)


def solution(mesh):
    placed = (
        P("ep", None),
        P(),
        P(None, "tp"),
        P(None, "tp"),
        P(None, "tp"),
        P(None, "tp"),
        P(),
        P(),
        P(),
        P("tp", None),
        P("ep", "tp", None, None),
        P("ep", "tp", None),
        P("ep", "tp"),
        P("ep", None),
        P("ep", None),
        P("ep", None, "tp"),
        P("ep", None, "tp"),
        P("ep", "tp", None),
        P("tp", "ep"),
        P("tp", "ep"),
        P("ep", "tp"),
        P(),
    )
    return jax.shard_map(
        local,
        mesh=mesh,
        in_specs=placed,
        out_specs=(P("ep", "tp"), P("ep", "tp", None, None), P("ep", "tp", None), P("ep", "tp")),
        check_vma=False,
    )
```

profile of v0, /device:TPU:0, one launch (start us, length us, event | category | flops | bytes accessed | tf_op | source)
XLA Modules:
  0.0 237.0 jit_solution(14512095781934341025)
XLA Ops:
  7.3 0.9 slice.14
  8.2 1.0 multiply_reduce_fusion
  9.2 1.6 convolution_convert_fusion.7
  10.9 1.1 fusion.44
  12.8 1.2 subtract_exponential_fusion
  14.1 1.6 convolution_convert_fusion.6
  15.8 1.6 convolution_convert_fusion.5
  18.7 3.7 %multiply_add_fusion = f32[32,2,128,128]{3,2,1,0:T(8,128)S(1)} fusion(f32[32,2,128,128]{3,2,1,0:T(8,128)} %param.32, f32[32,2,128]{2,1,0:T(2,128)S(1)} %reshape.112, f32[32,2,128]{2,1,0:T(2,128)S(1)} %get-tuple-element.20, f32[32,2]{1,0:T(8,128)S(1)} %copy.31), kind=kLoop, calls=%fused_computation | loop fusion | flops 3145728 | bytes 8454400 | tf_op jit(solution)/shard_map/add | solution.py:72
  22.5 2.0 copy-done.1
  25.3 0.9 convolution_convert_fusion
  26.8 0.9 fusion.56
  28.5 20.2 %reduce-scatter.4.cloned.1.call-done = bf16[32,512]{1,0:T(8,128)(2,1)} async-done(((bf16[32,2048]{1,0:T(8,128)(2,1)}), bf16[32,512]{1,0:T(8,128)(2,1)}) %reduce-scatter.4.cloned.1.call-update) | async-done | bytes 32784 | tf_op jit(solution)/shard_map/reduce_scatter | solution.py:83
  48.7 1.0 multiply_reduce_fusion.2
  49.7 5.8 %all-reduce = (f32[32]{0:T(128)S(1)}, f32[32]{0:T(128)S(1)}, f32[32]{0:T(128)S(1)}, f32[32]{0:T(128)S(1)}, f32[32]{0:T(128)S(1)}, /*index=5*/f32[32]{0:T(128)S(1)}) all-reduce(f32[32]{0:T(128)S(1)} %get-tuple-element.9, f32[32]{0:T(128)S(1)} %get-tuple-element.8, f32[32]{0:T(128)S(1)} %get-tuple-element.5, ...), channel_id=1, replica_groups=mesh['ep'=8,'tp'=4] {'tp'}, use_global_device_ids=true, to_apply=%region_3.4 | all-reduce | flops 192 | bytes 1536 | tf_op jit(solution)/shard_map/psum | solution.py:91
  55.5 0.9 multiply_convert_fusion.1
  56.3 31.2 %all_gather.7 = bf16[256,512]{1,0:T(8,128)(2,1)S(1)} all-gather(bf16[32,512]{1,0:T(8,128)(2,1)S(1)} %get-tuple-element.23), channel_id=1, replica_groups=mesh['ep'=8,'tp'=4] {'ep'}, dimensions={0}, use_global_device_ids=true | all-gather | bytes 294912 | tf_op jit(solution)/shard_map/all_gather | solution.py:110
  89.2 5.3 %all-to-all-start = ((bf16[8,16,512]{2,1,0:T(8,128)(2,1)}), bf16[8,16,512]{2,1,0:T(8,128)(2,1)S(1)}, u32[]{:S(2)}, u32[]{:S(2)}) async-start(bf16[8,16,512]{2,1,0:T(8,128)(2,1)} %bitcast.6), calls=%async_computation.1 | async-start | bytes 262144 | tf_op jit(solution)/shard_map/all_to_all | solution.py:145
  94.5 0.9 pad_maximum_fusion
  95.5 6.3 %all-to-all-done = bf16[8,16,512]{2,1,0:T(8,128)(2,1)S(1)} async-done(((bf16[8,16,512]{2,1,0:T(8,128)(2,1)}), bf16[8,16,512]{2,1,0:T(8,128)(2,1)S(1)}, u32[]{:S(2)}, u32[]{:S(2)}) %all-to-all-start) | async-done | bytes 131104 | tf_op jit(solution)/shard_map/all_to_all | solution.py:145
  101.8 9.2 %all_gather.6 = bf16[8,16,2048]{2,1,0:T(8,128)(2,1)S(1)} all-gather(bf16[8,16,512]{2,1,0:T(8,128)(2,1)S(1)} %all-to-all-done), channel_id=1, replica_groups=mesh['ep'=8,'tp'=4] {'tp'}, dimensions={2}, use_global_device_ids=true | all-gather | bytes 655360 | tf_op jit(solution)/shard_map/all_gather | solution.py:146
  111.0 2.8 %fusion.4 = f32[128,896]{1,0:T(8,128)S(1)} fusion(bf16[128,2048]{1,0:T(8,128)(2,1)S(1)} %bitcast.51, bf16[1,2048,896]{2,1,0:T(8,128)(2,1)} %param.37), kind=kOutput, calls=%fused_computation.5 | convolution fusion | flops 469762048 | bytes 4653056 | tf_op jit(solution)/shard_map/dot_general | solution.py:148
  113.9 5.5 %fusion.6 = bf16[128,2048]{1,0:T(8,128)(2,1)} fusion(bf16[1,896,2048]{2,1,0:T(8,128)(2,1)} %param.39, bf16[128,2048]{1,0:T(8,128)(2,1)S(1)} %bitcast.52, bf16[1,2048,896]{2,1,0:T(8,128)(2,1)} %param.38, f32[128,896]{1,0:T(8,128)S(1)} %fusion.4), kind=kOutput, calls=%fused_computation.7 | convolution fusion | flops 940474368 | bytes 8847360 | tf_op jit(solution)/shard_map/dot_general | solution.py:151
  119.4 13.2 %all-reduce.3.cloned.1.call-done = bf16[256,1408]{0,1:T(8,128)(2,1)} async-done(((bf16[256,1408]{0,1:T(8,128)(2,1)}), bf16[256,1408]{0,1:T(8,128)(2,1)}) %all-reduce.3.cloned.1.call-update) | async-done | bytes 720912 | tf_op jit(solution)/shard_map/psum | solution.py:118
  132.6 1.2 convert_element_type.94
  133.8 1.1 convolution_convert_fusion.3
  134.9 21.8 %reduce-scatter.6.cloned.1.call-done = bf16[128,512]{1,0:T(8,128)(2,1)} async-done(((bf16[128,2048]{1,0:T(8,128)(2,1)}), bf16[128,512]{1,0:T(8,128)(2,1)}) %reduce-scatter.6.cloned.1.call-update) | async-done | bytes 131088 | tf_op jit(solution)/shard_map/reduce_scatter | solution.py:152
  156.7 5.5 %all-to-all-start.1 = ((bf16[8,16,512]{2,1,0:T(8,128)(2,1)}), bf16[8,16,512]{2,1,0:T(8,128)(2,1)S(1)}, u32[]{:S(2)}, u32[]{:S(2)}) async-start(bf16[8,16,512]{2,1,0:T(8,128)(2,1)} %bitcast.62), calls=%async_computation.3 | async-start | bytes 262144 | tf_op jit(solution)/shard_map/all_to_all | solution.py:155
  162.4 7.2 %all-to-all-done.1 = bf16[8,16,512]{2,1,0:T(8,128)(2,1)S(1)} async-done(((bf16[8,16,512]{2,1,0:T(8,128)(2,1)}), bf16[8,16,512]{2,1,0:T(8,128)(2,1)S(1)}, u32[]{:S(2)}, u32[]{:S(2)}) %all-to-all-start.1) | async-done | bytes 131104 | tf_op jit(solution)/shard_map/all_to_all | solution.py:155
  169.8 52.6 %reduce-scatter.8.cloned.1.call-done = bf16[32,512]{1,0:T(8,128)(2,1)} async-done(((bf16[256,512]{1,0:T(8,128)(2,1)}), bf16[32,512]{1,0:T(8,128)(2,1)}) %reduce-scatter.8.cloned.1.call-update) | async-done | bytes 32784 | tf_op jit(solution)/shard_map/reduce_scatter | solution.py:121
  222.4 0.9 multiply_reduce_fusion.1
  223.3 5.7 %psum.63 = f32[32]{0:T(128)S(1)} all-reduce(f32[32]{0:T(128)S(1)} %multiply_reduce_fusion.1), channel_id=1, replica_groups=mesh['ep'=8,'tp'=4] {'tp'}, use_global_device_ids=true, to_apply=%region_22.23 | all-reduce | flops 32 | bytes 256 | tf_op jit(solution)/shard_map/psum | solution.py:169
  229.0 1.5 add_convert_fusion
  (65 shorter events, 6.6 us)
Async XLA Ops:
  7.2 18.1 %copy-start = (bf16[256,2048]{1,0:T(8,128)(2,1)S(1)}, bf16[256,2048]{1,0:T(8,128)(2,1)}, u32[]{:S(2)}) copy-start(bf16[256,2048]{1,0:T(8,128)(2,1)} %param.31) | copy-start | bytes 3145732
  7.2 11.2 %copy-start.2 = (bf16[32,2048]{1,0:T(8,128)(2,1)S(1)}, bf16[32,2048]{1,0:T(8,128)(2,1)}, u32[]{:S(2)}) copy-start(bf16[32,2048]{1,0:T(8,128)(2,1)} %param.22) | copy-start | bytes 393220
  7.2 10.3 %copy-start.6 = (f32[32,2,128]{2,1,0:T(2,128)S(1)}, f32[32,2,128]{2,1,0:T(2,128)}, u32[]{:S(2)}) copy-start(f32[32,2,128]{2,1,0:T(2,128)} %param.33) | copy-start | bytes 98308
  7.2 11.2 %copy-start.3 = (bf16[2048,256]{1,0:T(8,128)(2,1)S(1)}, bf16[2048,256]{1,0:T(8,128)(2,1)}, u32[]{:S(2)}) copy-start(bf16[2048,256]{1,0:T(8,128)(2,1)} %param.27) | copy-start | bytes 3145732
  7.2 41.5 %reduce-scatter.4.cloned.1.call-start = ((), (), s32[]{:S(2)}) async-start(), calls=%async_computation.5 | async-start | bytes 163840 | tf_op jit(solution)/shard_map/reduce_scatter | solution.py:83
  13.9 8.5 %copy-start.7 = (f32[32,2]{0,1:T(2,128)}, f32[32,2]{0,1:T(2,128)S(1)}, u32[]{:S(2)}) copy-start(f32[32,2]{0,1:T(2,128)S(1)} %get-tuple-element.22) | copy-start | bytes 772
  22.4 2.0 copy-start.1
  24.5 1.7 copy-start.9
  24.5 63.0 %copy-start.4 = (bf16[512,704]{0,1:T(8,128)(2,1)S(1)}, bf16[512,704]{0,1:T(8,128)(2,1)}, u32[]{:S(2)}) copy-start(bf16[512,704]{0,1:T(8,128)(2,1)} %param.41) | copy-start | bytes 2162692
  24.5 63.4 %copy-start.5 = (bf16[512,704]{0,1:T(8,128)(2,1)S(1)}, bf16[512,704]{0,1:T(8,128)(2,1)}, u32[]{:S(2)}) copy-start(bf16[512,704]{0,1:T(8,128)(2,1)} %param.40) | copy-start | bytes 2162692
  89.2 12.6 %all-to-all-start = ((bf16[8,16,512]{2,1,0:T(8,128)(2,1)}), bf16[8,16,512]{2,1,0:T(8,128)(2,1)S(1)}, u32[]{:S(2)}, u32[]{:S(2)}) async-start(bf16[8,16,512]{2,1,0:T(8,128)(2,1)} %bitcast.6), calls=%async_computation.1 | async-start | bytes 262144 | tf_op jit(solution)/shard_map/all_to_all | solution.py:145
  94.5 38.1 %all-reduce.3.cloned.1.call-start = ((), (), s32[]{:S(2)}) async-start(), calls=%async_computation.7 | async-start | bytes 1441792 | tf_op jit(solution)/shard_map/psum | solution.py:118
  95.5 61.3 %reduce-scatter.6.cloned.1.call-start = ((), (), s32[]{:S(2)}) async-start(), calls=%async_computation.6 | async-start | bytes 655360 | tf_op jit(solution)/shard_map/reduce_scatter | solution.py:152
  113.8 19.9 %copy-start.10 = (bf16[704,512]{1,0:T(8,128)(2,1)S(1)}, bf16[704,512]{1,0:T(8,128)(2,1)}, u32[]{:S(2)}) copy-start(bf16[704,512]{1,0:T(8,128)(2,1)} %param.42) | copy-start | bytes 2162692
  119.3 43.0 %copy-start.8 = (f32[32,2]{0,1:T(2,128)S(1)}, f32[32,2]{0,1:T(2,128)}, u32[]{:S(2)}) copy-start(f32[32,2]{0,1:T(2,128)} %param.36) | copy-start | bytes 772
  119.3 103.0 %reduce-scatter.8.cloned.1.call-start = ((), (), s32[]{:S(2)}) async-start(), calls=%async_computation.8 | async-start | bytes 294912 | tf_op jit(solution)/shard_map/reduce_scatter | solution.py:121
  156.7 12.9 %all-to-all-start.1 = ((bf16[8,16,512]{2,1,0:T(8,128)(2,1)}), bf16[8,16,512]{2,1,0:T(8,128)(2,1)S(1)}, u32[]{:S(2)}, u32[]{:S(2)}) async-start(bf16[8,16,512]{2,1,0:T(8,128)(2,1)} %bitcast.62), calls=%async_computation.3 | async-start | bytes 262144 | tf_op jit(solution)/shard_map/all_to_all | solution.py:155
Sparse Core Ops, SparseCore 0:
  26.3 22.3 reduce-scatter.3
  97.7 34.8 all-reduce.2
  135.0 21.6 reduce-scatter.5
  159.9 62.4 reduce-scatter.7
where the time goes:
time: 238 us; the launch traced here: 237 us
  waiting for transfers between devices  121 us (51%)
  blocking collectives  51.8 us (22%)
  matrix products  20.2 us (8%)
  between operations  14.1 us (6%)
  other arithmetic  13.3 us (6%)
  starting transfers between devices  11 us (5%)
  local copies, waits for them, and re-layouts  5.31 us (2%)
    reduce_scatter x1, waiting for transfers between devices, local(): lax.psum_scatter(jnp.dot(dense_hidden, dense_down, preferred_element_type...  52.6 us
    all_gather x1, blocking collectives, local(): rows_in = lax.all_gather(normed, 'ep', axis=0, tiled=True)  31.2 us
    reduce_scatter x1, waiting for transfers between devices, local(): lax.psum_scatter(partial_out.astype(jnp.bfloat16), 'tp', scatter_dimensio...  21.8 us
    reduce_scatter x1, waiting for transfers between devices, local(): lax.psum_scatter(branch_terms.astype(jnp.bfloat16), 'tp', scatter_dimensi...  20.2 us
    psum x1, waiting for transfers between devices, local(): lax.psum(dense_pre.astype(jnp.bfloat16), 'tp').astype(jnp.float32)  13.2 us
    all_gather x1, blocking collectives, local(): full_rows = lax.all_gather(arrived, 'tp', axis=2, tiled=True)  9.21 us
    all_to_all x1, waiting for transfers between devices, local(): lax.all_to_all(summed_out.reshape(arrived.shape), 'ep', split_axis=0, con...  7.21 us
    all_to_all x1, waiting for transfers between devices, local(): lax.all_to_all(outgoing, 'ep', split_axis=0, concat_axis=0, tiled=True)  6.31 us
  transfers between devices with their start and end apart: 6, of which 6 were waited for; matrix products, arithmetic and copies ran while one was open for 6% of the time, Pallas kernels for 0%

commit v1 on v0

--- a/solution.py
+++ b/solution.py
@@ -107,7 +107,20 @@
     mix_gate = jax.nn.sigmoid(scale_two * gate_dot)
     residual = settle(residual_f)
     normed = (residual_f * scale_two[:, None] * gain_rows[2]).astype(jnp.bfloat16)
-    rows_in = lax.all_gather(normed, "ep", axis=0, tiled=True)
+    z2, state_now, before = (lax.axis_size("ep"), lax.axis_index("ep"), normed.shape[0])
+    block_next, frame_out = (normed, 1)
+    while frame_out < z2:
+        block_next = jnp.concatenate(
+            [
+                block_next,
+                lax.ppermute(
+                    block_next, "ep", perm=[(k0, (k0 - frame_out) % z2) for k0 in range(z2)]
+                ),
+            ],
+            axis=0,
+        )
+        frame_out = 2 * frame_out
+    rows_in = jnp.roll(block_next, state_now * before, axis=0)
     dense_pre = jnp.concatenate(
         [
             jnp.dot(rows_in, dense_gate, preferred_element_type=jnp.float32),

time: 238 us -> 221 us (0.929)
  blocking collectives: 51.8 us -> 17.9 us
  starting transfers between devices: 11 us -> 19.9 us
  waiting for transfers between devices: 121 us -> 128 us
    all_gather x1 -> x0, blocking collectives: 31.2 us -> none  [local(): rows_in = lax.all_gather(normed, 'ep', axis=0, tiled=True)]
    ppermute x0 -> x3, starting transfers between devices: none -> 8.84 us  [local(): lax.ppermute(block_next, 'ep', perm=[(k0, (k0 - frame_out) % z2) for k0 i...]
    ppermute x0 -> x3, waiting for transfers between devices: none -> 8.51 us  [local(): lax.ppermute(block_next, 'ep', perm=[(k0, (k0 - frame_out) % z2) for k0 i...]
    all_to_all x1, waiting for transfers between devices: 6.31 us -> 0.01 us  [local(): lax.all_to_all(outgoing, 'ep', split_axis=0, concat_axis=0, tiled=True)]
    psum x1, waiting for transfers between devices: 13.2 us -> 18.3 us  [local(): lax.psum(dense_pre.astype(jnp.bfloat16), 'tp').astype(jnp.float32)]
    all_gather x1, blocking collectives: 9.21 us -> 6.5 us  [local(): full_rows = lax.all_gather(arrived, 'tp', axis=2, tiled=True)]
  transfers between devices with their start and end apart: 6 -> 9, of which waited for: 6 -> 7; matrix products, arithmetic and copies ran while one was open for 6% -> 8% of each run, Pallas kernels for 0% -> 0%
where the time goes in v1:
time: 221 us; the launch traced here: 220 us
  waiting for transfers between devices  128 us (58%)
  matrix products  21.2 us (10%)
  starting transfers between devices  19.9 us (9%)
  blocking collectives  17.9 us (8%)
  between operations  14.1 us (6%)
  other arithmetic  14 us (6%)
  local copies, waits for them, and re-layouts  5.36 us (2%)
    reduce_scatter x1, waiting for transfers between devices, local(): lax.psum_scatter(jnp.dot(dense_hidden, dense_down, preferred_element_type...  52.6 us
    reduce_scatter x1, waiting for transfers between devices, local(): lax.psum_scatter(partial_out.astype(jnp.bfloat16), 'tp', scatter_dimensio...  20.7 us
    reduce_scatter x1, waiting for transfers between devices, local(): lax.psum_scatter(branch_terms.astype(jnp.bfloat16), 'tp', scatter_dimensi...  20.3 us
    psum x1, waiting for transfers between devices, local(): lax.psum(dense_pre.astype(jnp.bfloat16), 'tp').astype(jnp.float32)  18.3 us
    ppermute x3, starting transfers between devices, local(): lax.ppermute(block_next, 'ep', perm=[(k0, (k0 - frame_out) % z2) for k0 i...  8.84 us
    ppermute x3, waiting for transfers between devices, local(): lax.ppermute(block_next, 'ep', perm=[(k0, (k0 - frame_out) % z2) for k0 i...  8.51 us
    all_to_all x1, waiting for transfers between devices, local(): lax.all_to_all(summed_out.reshape(arrived.shape), 'ep', split_axis=0, con...  7.23 us
    all_gather x1, blocking collectives, local(): full_rows = lax.all_gather(arrived, 'tp', axis=2, tiled=True)  6.5 us
  transfers between devices with their start and end apart: 9, of which 7 were waited for; matrix products, arithmetic and copies ran while one was open for 8% of the time, Pallas kernels for 0%

profile of v1, /device:TPU:0, one launch (start us, length us, event | category | flops | bytes accessed | tf_op | source)
XLA Modules:
  0.0 220.2 jit_solution(6210317358927325782)
XLA Ops:
  8.2 1.0 multiply_reduce_fusion
  9.2 1.6 convolution_convert_fusion.7
  10.9 1.6 convolution_convert_fusion.5
  12.6 1.1 fusion.46
  14.4 1.2 subtract_exponential_fusion
  15.7 1.6 convolution_convert_fusion.6
  18.7 3.7 %multiply_add_fusion = f32[32,2,128,128]{3,2,1,0:T(8,128)S(1)} fusion(f32[32,2,128,128]{3,2,1,0:T(8,128)} %param.32, f32[32,2,128]{2,1,0:T(2,128)S(1)} %reshape.112, f32[32,2,128]{2,1,0:T(2,128)S(1)} %get-tuple-element.22, f32[32,2]{1,0:T(8,128)S(1)} %copy.31), kind=kLoop, calls=%fused_computation | loop fusion | flops 3145728 | bytes 8454400 | tf_op jit(solution)/shard_map/add | solution.py:72
  22.5 2.0 copy-done.1
  25.2 0.9 convolution_convert_fusion
  28.4 20.3 %reduce-scatter.4.cloned.1.call-done = bf16[32,512]{1,0:T(8,128)(2,1)} async-done(((bf16[32,2048]{1,0:T(8,128)(2,1)}), bf16[32,512]{1,0:T(8,128)(2,1)}) %reduce-scatter.4.cloned.1.call-update) | async-done | bytes 32784 | tf_op jit(solution)/shard_map/reduce_scatter | solution.py:83
  48.7 1.0 multiply_reduce_fusion.2
  49.7 5.8 %all-reduce = (f32[32]{0:T(128)S(1)}, f32[32]{0:T(128)S(1)}, f32[32]{0:T(128)S(1)}, f32[32]{0:T(128)S(1)}, f32[32]{0:T(128)S(1)}, /*index=5*/f32[32]{0:T(128)S(1)}) all-reduce(f32[32]{0:T(128)S(1)} %get-tuple-element.9, f32[32]{0:T(128)S(1)} %get-tuple-element.8, f32[32]{0:T(128)S(1)} %get-tuple-element.5, ...), channel_id=1, replica_groups=mesh['ep'=8,'tp'=4] {'tp'}, use_global_device_ids=true, to_apply=%region_3.4 | all-reduce | flops 192 | bytes 1536 | tf_op jit(solution)/shard_map/psum | solution.py:91
  56.3 4.4 %collective-permute-start = (bf16[32,512]{1,0:T(8,128)(2,1)S(1)}, bf16[32,512]{1,0:T(8,128)(2,1)S(1)}, u32[]{:S(2)}, u32[]{:S(2)}) collective-permute-start(bf16[32,512]{1,0:T(8,128)(2,1)S(1)} %get-tuple-element.19), channel_id=1, source_target_pairs={{0,28},{4,0},{8,4},{12,8},{16,12},{20,16},{24,20},{28,24},{1,29},{... | collective-permute-start | bytes 98312 | tf_op jit(solution)/shard_map/ppermute | solution.py:116
  60.8 1.5 collective-permute-done
  63.0 1.4 collective-permute-start.1
  65.3 5.4 %all-to-all-start = ((bf16[8,16,512]{2,1,0:T(8,128)(2,1)}), bf16[8,16,512]{2,1,0:T(8,128)(2,1)S(1)}, u32[]{:S(2)}, u32[]{:S(2)}) async-start(bf16[8,16,512]{2,1,0:T(8,128)(2,1)} %bitcast.51), calls=%async_computation.1 | async-start | bytes 262144 | tf_op jit(solution)/shard_map/all_to_all | solution.py:158
  70.7 2.9 %collective-permute-start.2 = (bf16[128,512]{1,0:T(8,128)(2,1)S(1)}, bf16[128,512]{1,0:T(8,128)(2,1)S(1)}, u32[]{:S(2)}, u32[]{:S(2)}) collective-permute-start(bf16[128,512]{1,0:T(8,128)(2,1)S(1)} %pad_maximum_fusion.1), channel_id=1, source_target_pairs={{0,16},{4,20},{8,24},{12,28},{16,0},{20,4},{24,8},{28,12},{1,17},{... | collective-permute-start | bytes 393224 | tf_op jit(solution)/shard_map/ppermute | solution.py:116
  73.7 7.0 %collective-permute-done.2 = bf16[128,512]{1,0:T(8,128)(2,1)S(1)} collective-permute-done((bf16[128,512]{1,0:T(8,128)(2,1)S(1)}, bf16[128,512]{1,0:T(8,128)(2,1)S(1)}, u32[]{:S(2)}, u32[]{:S(2)}) %collective-permute-start.2) | collective-permute-done | bytes 131104 | tf_op jit(solution)/shard_map/ppermute | solution.py:116
  81.6 0.9 pad_maximum_fusion
  82.6 6.5 %all_gather.3 = bf16[8,16,2048]{2,1,0:T(8,128)(2,1)S(1)} all-gather(bf16[8,16,512]{2,1,0:T(8,128)(2,1)S(1)} %all-to-all-done), channel_id=1, replica_groups=mesh['ep'=8,'tp'=4] {'tp'}, dimensions={2}, use_global_device_ids=true | all-gather | bytes 655360 | tf_op jit(solution)/shard_map/all_gather | solution.py:159
  89.1 2.8 %fusion.4 = f32[128,896]{1,0:T(8,128)S(1)} fusion(bf16[128,2048]{1,0:T(8,128)(2,1)S(1)} %bitcast.49, bf16[1,2048,896]{2,1,0:T(8,128)(2,1)} %param.37), kind=kOutput, calls=%fused_computation.5 | convolution fusion | flops 469762048 | bytes 4653056 | tf_op jit(solution)/shard_map/dot_general | solution.py:161
  91.9 5.4 %fusion.6 = bf16[128,2048]{1,0:T(8,128)(2,1)} fusion(bf16[1,896,2048]{2,1,0:T(8,128)(2,1)} %param.39, bf16[128,2048]{1,0:T(8,128)(2,1)S(1)} %bitcast.50, bf16[1,2048,896]{2,1,0:T(8,128)(2,1)} %param.38, f32[128,896]{1,0:T(8,128)S(1)} %fusion.4), kind=kOutput, calls=%fused_computation.7 | convolution fusion | flops 940474368 | bytes 8847360 | tf_op jit(solution)/shard_map/dot_general | solution.py:164
  97.4 18.3 %all-reduce.3.cloned.1.call-done = bf16[256,1408]{0,1:T(8,128)(2,1)} async-done(((bf16[256,1408]{0,1:T(8,128)(2,1)}), bf16[256,1408]{0,1:T(8,128)(2,1)}) %all-reduce.3.cloned.1.call-update) | async-done | bytes 720912 | tf_op jit(solution)/shard_map/psum | solution.py:131
  115.7 1.2 convert_element_type.94
  116.9 2.2 %convolution_convert_fusion.3 = bf16[256,512]{1,0:T(8,128)(2,1)} fusion(bf16[704,512]{1,0:T(8,128)(2,1)} %param.42, f32[256,1408]{0,1:T(8,128)S(1)} %convert_element_type.94), kind=kOutput, calls=%fused_computation.12 | convolution fusion | flops 185761792 | bytes 2424832 | tf_op jit(solution)/shard_map/dot_general | solution.py:135
  119.2 20.7 %reduce-scatter.6.cloned.1.call-done = bf16[128,512]{1,0:T(8,128)(2,1)} async-done(((bf16[128,2048]{1,0:T(8,128)(2,1)}), bf16[128,512]{1,0:T(8,128)(2,1)}) %reduce-scatter.6.cloned.1.call-update) | async-done | bytes 131088 | tf_op jit(solution)/shard_map/reduce_scatter | solution.py:165
  139.9 5.5 %all-to-all-start.1 = ((bf16[8,16,512]{2,1,0:T(8,128)(2,1)}), bf16[8,16,512]{2,1,0:T(8,128)(2,1)S(1)}, u32[]{:S(2)}, u32[]{:S(2)}) async-start(bf16[8,16,512]{2,1,0:T(8,128)(2,1)} %bitcast.61), calls=%async_computation.3 | async-start | bytes 262144 | tf_op jit(solution)/shard_map/all_to_all | solution.py:168
  145.6 7.2 %all-to-all-done.1 = bf16[8,16,512]{2,1,0:T(8,128)(2,1)S(1)} async-done(((bf16[8,16,512]{2,1,0:T(8,128)(2,1)}), bf16[8,16,512]{2,1,0:T(8,128)(2,1)S(1)}, u32[]{:S(2)}, u32[]{:S(2)}) %all-to-all-start.1) | async-done | bytes 131104 | tf_op jit(solution)/shard_map/all_to_all | solution.py:168
  153.0 52.6 %reduce-scatter.8.cloned.1.call-done = bf16[32,512]{1,0:T(8,128)(2,1)} async-done(((bf16[256,512]{1,0:T(8,128)(2,1)}), bf16[32,512]{1,0:T(8,128)(2,1)}) %reduce-scatter.8.cloned.1.call-update) | async-done | bytes 32784 | tf_op jit(solution)/shard_map/reduce_scatter | solution.py:134
  205.6 0.9 multiply_reduce_fusion.1
  206.5 5.7 %psum.63 = f32[32]{0:T(128)S(1)} all-reduce(f32[32]{0:T(128)S(1)} %multiply_reduce_fusion.1), channel_id=1, replica_groups=mesh['ep'=8,'tp'=4] {'tp'}, use_global_device_ids=true, to_apply=%region_22.23 | all-reduce | flops 32 | bytes 256 | tf_op jit(solution)/shard_map/psum | solution.py:182
  212.2 1.5 add_convert_fusion
  (84 shorter events, 10.0 us)
Async XLA Ops:
  7.2 18.1 %copy-start = (bf16[256,2048]{1,0:T(8,128)(2,1)S(1)}, bf16[256,2048]{1,0:T(8,128)(2,1)}, u32[]{:S(2)}) copy-start(bf16[256,2048]{1,0:T(8,128)(2,1)} %param.31) | copy-start | bytes 3145732
  7.2 11.2 %copy-start.2 = (bf16[32,2048]{1,0:T(8,128)(2,1)S(1)}, bf16[32,2048]{1,0:T(8,128)(2,1)}, u32[]{:S(2)}) copy-start(bf16[32,2048]{1,0:T(8,128)(2,1)} %param.22) | copy-start | bytes 393220
  7.2 10.3 %copy-start.7 = (f32[32,2,128]{2,1,0:T(2,128)S(1)}, f32[32,2,128]{2,1,0:T(2,128)}, u32[]{:S(2)}) copy-start(f32[32,2,128]{2,1,0:T(2,128)} %param.33) | copy-start | bytes 98308
  7.2 11.2 %copy-start.3 = (bf16[2048,256]{1,0:T(8,128)(2,1)S(1)}, bf16[2048,256]{1,0:T(8,128)(2,1)}, u32[]{:S(2)}) copy-start(bf16[2048,256]{1,0:T(8,128)(2,1)} %param.27) | copy-start | bytes 3145732
  7.2 41.5 %reduce-scatter.4.cloned.1.call-start = ((), (), s32[]{:S(2)}) async-start(), calls=%async_computation.5 | async-start | bytes 163840 | tf_op jit(solution)/shard_map/reduce_scatter | solution.py:83
  15.6 6.8 %copy-start.8 = (f32[32,2]{0,1:T(2,128)}, f32[32,2]{0,1:T(2,128)S(1)}, u32[]{:S(2)}) copy-start(f32[32,2]{0,1:T(2,128)S(1)} %get-tuple-element.24) | copy-start | bytes 772
  22.4 2.0 copy-start.1
  24.5 1.7 copy-start.12
  24.5 56.3 %copy-start.4 = (bf16[512,704]{0,1:T(8,128)(2,1)S(1)}, bf16[512,704]{0,1:T(8,128)(2,1)}, u32[]{:S(2)}) copy-start(bf16[512,704]{0,1:T(8,128)(2,1)} %param.41) | copy-start | bytes 2162692
  25.1 56.1 %copy-start.5 = (bf16[512,704]{0,1:T(8,128)(2,1)S(1)}, bf16[512,704]{0,1:T(8,128)(2,1)}, u32[]{:S(2)}) copy-start(bf16[512,704]{0,1:T(8,128)(2,1)} %param.40) | copy-start | bytes 2162692
  56.3 6.0 %collective-permute-start = (bf16[32,512]{1,0:T(8,128)(2,1)S(1)}, bf16[32,512]{1,0:T(8,128)(2,1)S(1)}, u32[]{:S(2)}, u32[]{:S(2)}) collective-permute-start(bf16[32,512]{1,0:T(8,128)(2,1)S(1)} %get-tuple-element.19), channel_id=1, source_target_pairs={{0,28},{4,0},{8,4},{12,8},{16,12},{20,16},{24,20},{28,24},{1,29},{... | collective-permute-start | bytes 98312 | tf_op jit(solution)/shard_map/ppermute | solution.py:116
  60.8 4.5 %copy-start.10 = (s32[64]{0:T(128)}, s32[64]{0:T(128)S(1)}, u32[]{:S(2)}) copy-start(s32[64]{0:T(128)S(1)} %add_add_fusion) | copy-start | bytes 772
  63.0 7.7 %collective-permute-start.1 = (bf16[64,512]{1,0:T(8,128)(2,1)}, bf16[64,512]{1,0:T(8,128)(2,1)S(1)}, u32[]{:S(2)}, u32[]{:S(2)}) collective-permute-start(bf16[64,512]{1,0:T(8,128)(2,1)} %pad_maximum_fusion.2), channel_id=1, source_target_pairs={{0,24},{4,28},{8,0},{12,4},{16,8},{20,12},{24,16},{28,20},{1,25},{... | collective-permute-start | bytes 196616 | tf_op jit(solution)/shard_map/ppermute | solution.py:116
  65.3 17.3 %all-to-all-start = ((bf16[8,16,512]{2,1,0:T(8,128)(2,1)}), bf16[8,16,512]{2,1,0:T(8,128)(2,1)S(1)}, u32[]{:S(2)}, u32[]{:S(2)}) async-start(bf16[8,16,512]{2,1,0:T(8,128)(2,1)} %bitcast.51), calls=%async_computation.1 | async-start | bytes 262144 | tf_op jit(solution)/shard_map/all_to_all | solution.py:158
  70.7 45.1 %all-reduce.3.cloned.1.call-start = ((), (), s32[]{:S(2)}) async-start(), calls=%async_computation.7 | async-start | bytes 1441792 | tf_op jit(solution)/shard_map/psum | solution.py:131
  70.7 9.9 %collective-permute-start.2 = (bf16[128,512]{1,0:T(8,128)(2,1)S(1)}, bf16[128,512]{1,0:T(8,128)(2,1)S(1)}, u32[]{:S(2)}, u32[]{:S(2)}) collective-permute-start(bf16[128,512]{1,0:T(8,128)(2,1)S(1)} %pad_maximum_fusion.1), channel_id=1, source_target_pairs={{0,16},{4,20},{8,24},{12,28},{16,0},{20,4},{24,8},{28,12},{1,17},{... | collective-permute-start | bytes 393224 | tf_op jit(solution)/shard_map/ppermute | solution.py:116
  82.5 57.4 %reduce-scatter.6.cloned.1.call-start = ((), (), s32[]{:S(2)}) async-start(), calls=%async_computation.6 | async-start | bytes 655360 | tf_op jit(solution)/shard_map/reduce_scatter | solution.py:165
  91.8 5.5 %copy-start.9 = (f32[32,2]{0,1:T(2,128)S(1)}, f32[32,2]{0,1:T(2,128)}, u32[]{:S(2)}) copy-start(f32[32,2]{0,1:T(2,128)} %param.36) | copy-start | bytes 772
  91.8 5.5 %copy-start.11 = (s32[64]{0:T(128)S(1)}, s32[64]{0:T(128)}, u32[]{:S(2)}) copy-start(s32[64]{0:T(128)} %copy-done.10) | copy-start | bytes 772
  97.2 108.4 %reduce-scatter.8.cloned.1.call-start = ((), (), s32[]{:S(2)}) async-start(), calls=%async_computation.8 | async-start | bytes 294912 | tf_op jit(solution)/shard_map/reduce_scatter | solution.py:134
  97.4 48.1 %copy-start.6 = (bf16[32,512]{1,0:T(8,128)(2,1)S(1)}, bf16[32,512]{1,0:T(8,128)(2,1)}, u32[]{:S(2)}) copy-start(bf16[32,512]{1,0:T(8,128)(2,1)} %reduce-scatter.4.cloned.1.call-done) | copy-start | bytes 98308
  139.9 12.9 %all-to-all-start.1 = ((bf16[8,16,512]{2,1,0:T(8,128)(2,1)}), bf16[8,16,512]{2,1,0:T(8,128)(2,1)S(1)}, u32[]{:S(2)}, u32[]{:S(2)}) async-start(bf16[8,16,512]{2,1,0:T(8,128)(2,1)} %bitcast.61), calls=%async_computation.3 | async-start | bytes 262144 | tf_op jit(solution)/shard_map/all_to_all | solution.py:168
Sparse Core Ops, SparseCore 0:
  26.3 22.3 reduce-scatter.3
  82.6 33.0 all-reduce.2
  118.2 21.6 reduce-scatter.5
  143.1 62.4 reduce-scatter.7
